TPU v7x, 256 devices: a whole 4x4x8 slice. The times are simulated.
256 devices in a mesh: ep: 64 (over z, y, core), tp: 4 (over x).
Axes of the slice: x: 4, y: 4, z: 8, core: 2. Of those that a mesh axis runs over, the one named last changes fastest.
Arguments:
- mixer_input: bfloat16 [32768, 2048], P('ep'), may hold values from -6 to 6
- mixer_gain: bfloat16 [2048], replicated, may hold values from 0.099609375 to 1.8984375
- pool_in: bfloat16 [2048, 1024], P(None, 'tp'), may hold values from -0.125 to 0.125
- pool_map: bfloat16 [4, 256, 256], P('tp'), may hold values from -0.375 to 0.375
- pool_scale: bfloat16 [1024], P('tp'), may hold values from 0.099609375 to 1.8984375
- pool_out: bfloat16 [1024, 2048], P('tp'), may hold values from -0.1875 to 0.1875
- expert_input: bfloat16 [24576, 2048], P('ep'), may hold values from -6 to 6
- expert_gain: bfloat16 [2048], replicated, may hold values from 0.099609375 to 1.8984375
- group_router: bfloat16 [2048, 4], replicated, may hold values from -0.125 to 0.125
- expert_router: bfloat16 [2048, 64], replicated, may hold values from -0.125 to 0.125
- routes: int32 [24576, 2], P('ep'), may hold values from 0 to 63, all different within a row; in each aligned block of 96 rows (0 to 95, 96 to 191, ...) at most 6 rows name the same one
- gate_weight: bfloat16 [64, 2048, 1024], P('ep', None, 'tp'), may hold values from -0.125 to 0.125
- up_weight: bfloat16 [64, 2048, 1024], P('ep', None, 'tp'), may hold values from -0.125 to 0.125
- down_weight: bfloat16 [64, 1024, 2048], P('ep', 'tp'), may hold values from -0.1875 to 0.1875
Outputs:
- mixer_output: bfloat16 [32768, 2048], P(('ep', 'tp'))
- expert_output: bfloat16 [24576, 2048], P(('ep', 'tp'))
Inputs may be any that keep to these rules, and one draw needn't show every extreme that they name: `routes`: each row names two different experts. In each aligned block of 96 rows no expert is named more than 6 times, a bound that some block reaches.
All inputs are finite; a program needn't handle non-finite values.
Results may differ from a plain program's by a relative error of at most 0.01.
Values may be sent and summed in bfloat16 or wider, within the bound.
No kernel may reach another device: no remote copies, remote signals or barrier semaphores. Data moves between devices by JAX's collectives and lax.ppermute only.
A program may use at most 64 MiB of HBM per device.

v0:
```python
import jax
import jax.numpy as jnp
from jax import lax
from jax.sharding import PartitionSpec as P

RIM = 15
EPS = 1e-06


def passed_along(value, axis, steps):
    count = lax.axis_size(axis)
    leading, last = (max(0, -steps), min(count, count - steps))
    return lax.ppermute(value, axis, [(source, source + steps) for source in range(leading, last)])


def norm_rows(values, gain):
    floats = values.astype(jnp.float32)
    scale = lax.rsqrt(jnp.mean(floats * floats, axis=-1, keepdims=True) + EPS)
    return (floats * scale * gain.astype(jnp.float32)).astype(jnp.bfloat16)


def route_weights(rows, group_router, expert_router, route_rows):
    group_logits = jnp.dot(rows, group_router, preferred_element_type=jnp.float32)
    expert_logits = jnp.dot(rows, expert_router, preferred_element_type=jnp.float32)
    groups = group_logits.shape[1]
    experts = expert_logits.shape[1]
    member = (
        jnp.arange(experts, dtype=jnp.int32)[:, None] // (experts // groups)
        == jnp.arange(groups, dtype=jnp.int32)[None, :]
    ).astype(jnp.float32)
    group_exp = jnp.exp(group_logits)
    group_prob = group_exp / jnp.sum(group_exp, axis=1, keepdims=True)
    expert_exp = jnp.exp(expert_logits)
    within = jnp.dot(expert_exp, member, precision=lax.Precision.HIGHEST)
    prob = expert_exp * jnp.dot(group_prob / within, member.T, precision=lax.Precision.HIGHEST)
    chosen = (route_rows[:, :, None] == jnp.arange(experts, dtype=jnp.int32)[None, None, :]).astype(
        jnp.float32
    )
    picked = jnp.sum(chosen * prob[:, None, :], axis=2)
    return picked / jnp.sum(picked, axis=1, keepdims=True)


def mixer_half(mixer_input, mixer_gain, pool_in, pool_map, pool_scale, pool_out):
    normed = norm_rows(mixer_input, mixer_gain)
    pooled_in = jnp.dot(normed, pool_in, preferred_element_type=jnp.float32).astype(jnp.bfloat16)
    local_rows = pooled_in.shape[0]
    groups_here = pool_map.shape[0]
    channels = pool_map.shape[1]
    border = passed_along(pooled_in[local_rows - RIM :], "ep", 1)
    padded = jnp.concatenate([border, pooled_in], axis=0).astype(jnp.float32)
    padded = padded.reshape(local_rows + RIM, groups_here, channels)
    leading = lax.axis_index("tp") * groups_here
    windows = jnp.left_shift(jnp.int32(2), leading + jnp.arange(groups_here, dtype=jnp.int32))
    window_sum = jnp.zeros((local_rows, groups_here, channels), jnp.float32)
    for offset in range(RIM + 1):
        active = (offset < windows).astype(jnp.float32)
        window_sum = (
            window_sum + padded[RIM - offset : RIM - offset + local_rows] * active[None, :, None]
        )
    position = lax.axis_index("ep") * local_rows + jnp.arange(local_rows, dtype=jnp.int32)
    counts_here = jnp.minimum(position[:, None] + 1, windows[None, :]).astype(jnp.float32)
    pooled = (window_sum / counts_here[:, :, None] - padded[RIM:]).astype(jnp.bfloat16)
    mapped = jnp.einsum("tgc,gce->tge", pooled, pool_map, preferred_element_type=jnp.float32)
    mixed_rows = (
        mapped.reshape(local_rows, groups_here * channels) * pool_scale.astype(jnp.float32)
    ).astype(jnp.bfloat16)
    return lax.psum_scatter(
        jnp.dot(mixed_rows, pool_out, preferred_element_type=jnp.float32).astype(jnp.bfloat16),
        "tp",
        scatter_dimension=0,
        tiled=True,
    )


def slot_positions(route_rows, blocks, experts):
    flat = route_rows.reshape(blocks, -1)
    onehot = (flat[:, :, None] == jnp.arange(experts, dtype=jnp.int32)[None, None, :]).astype(
        jnp.int32
    )
    before = jnp.cumsum(onehot, axis=1) - onehot
    return (jnp.sum(before * onehot, axis=2), flat)


def dispatch_rows(normed, route_rows, blocks, slots_each, experts):
    block_len = normed.shape[0] // blocks
    positions, flat = slot_positions(route_rows, blocks, experts)
    block_index = jnp.arange(blocks, dtype=jnp.int32)[:, None]
    slot_index = block_index * slots_each + positions
    token_index = block_index * block_len + jnp.arange(2 * block_len, dtype=jnp.int32)[None, :] // 2
    table = jnp.full((blocks * slots_each, experts), -1, jnp.int32)
    table = table.at[slot_index.reshape(-1), flat.reshape(-1)].set(token_index.reshape(-1))
    fetched = normed[jnp.maximum(table, 0)]
    return jnp.where((table >= 0)[:, :, None], fetched, jnp.zeros_like(fetched))


def expert_half(
    expert_input,
    expert_gain,
    group_router,
    expert_router,
    routes,
    gate_weight,
    up_weight,
    down_weight,
):
    normed = norm_rows(expert_input, expert_gain)
    tp_count = lax.axis_size("tp")
    tp_place = lax.axis_index("tp")
    experts = expert_router.shape[1]
    block_len = normed.shape[0] // tp_count
    slots_each = 4 * block_len // experts
    own_rows = lax.dynamic_slice_in_dim(normed, tp_place * block_len, block_len, 0)
    own_routes = lax.dynamic_slice_in_dim(routes, tp_place * block_len, block_len, 0)
    sending = dispatch_rows(own_rows, own_routes, 1, slots_each, experts)
    arrived = lax.all_to_all(sending, "ep", split_axis=1, concat_axis=1, tiled=True)
    received = lax.all_gather(arrived, "tp", axis=0, tiled=True)
    held = gate_weight.shape[0]
    model = received.shape[2]
    down_whole = lax.all_gather(down_weight, "tp", axis=1, tiled=True)
    all_slots = received.reshape(received.shape[0], -1, held, model)
    gate = jnp.einsum("csed,edh->cseh", all_slots, gate_weight, preferred_element_type=jnp.float32)
    upward = jnp.einsum("csed,edh->cseh", all_slots, up_weight, preferred_element_type=jnp.float32)
    hidden = (jax.nn.silu(gate) * upward).astype(jnp.bfloat16)
    swapped = lax.all_to_all(hidden, "tp", split_axis=0, concat_axis=3, tiled=True)
    hid_part = hidden.shape[3]
    total = jnp.zeros((swapped.shape[0], swapped.shape[1], held, model), jnp.float32)
    for part in range(tp_count):
        partial_value = jnp.einsum(
            "cseh,ehd->csed",
            swapped[:, :, :, part * hid_part : (part + 1) * hid_part],
            down_whole[:, part * hid_part : (part + 1) * hid_part],
            preferred_element_type=jnp.float32,
        ).astype(jnp.bfloat16)
        partial_value = lax.optimization_barrier(partial_value)
        total = total + partial_value.astype(jnp.float32)
    summed = total.astype(jnp.bfloat16).reshape(slots_each, -1, model)
    returned = lax.all_to_all(summed, "ep", split_axis=1, concat_axis=1, tiled=True)
    positions, flat = slot_positions(own_routes, 1, experts)
    lookup = positions[0] * experts + flat[0]
    picked = (
        returned.reshape(slots_each * experts, model)[lookup]
        .astype(jnp.float32)
        .reshape(block_len, 2, model)
    )
    weights = route_weights(own_rows, group_router, expert_router, own_routes)
    return jnp.sum(picked * weights[:, :, None], axis=1).astype(jnp.bfloat16)


def on_device(
    mixer_input,
    mixer_gain,
    pool_in,
    pool_map,
    pool_scale,
    pool_out,
    expert_input,
    expert_gain,
    group_router,
    expert_router,
    routes,
    gate_weight,
    up_weight,
    down_weight,
):
    mixer_output = mixer_half(mixer_input, mixer_gain, pool_in, pool_map, pool_scale, pool_out)
    expert_output = expert_half(
        expert_input,
        expert_gain,
        group_router,
        expert_router,
        routes,
        gate_weight,
        up_weight,
        down_weight,
    )
    return (mixer_output, expert_output)


def solution(mesh):
    return jax.shard_map(
        on_device,
        mesh=mesh,
        in_specs=(
            P("ep", None),
            P(),
            P(None, "tp"),
            P("tp", None, None),
            P("tp"),
            P("tp", None),
            P("ep", None),
            P(),
            P(),
            P(),
            P("ep", None),
            P("ep", None, "tp"),
            P("ep", None, "tp"),
            P("ep", "tp", None),
        ),
        out_specs=(P(("ep", "tp"), None), P(("ep", "tp"), None)),
        check_vma=False,
    )
```

profile of v0, /device:TPU:8, one launch (start us, length us, event | category | flops | bytes accessed | tf_op | source)
XLA Modules:
  0.0 302.8 jit_solution(5306408200580199578)
XLA Ops:
  9.5 1.8 multiply_reduce_fusion
  11.3 2.0 convert_element_type.227
  13.9 9.3 %scatter_fusion = s32[6,64]{1,0:T(8,128)S(1)} fusion(s32[6,64]{1,0:T(8,128)S(1)} %broadcast_in_dim.11, s32[192]{0:T(256)S(1)} %bitcast.129, s32[192]{0:T(256)S(1)} %and_select_fusion.1), kind=kCustom, calls=%fused_computation.2 | custom fusion | bytes 3840 | tf_op jit(solution)/shard_map/scatter | solution.py:91
  24.8 2.5 gather_fusion
  28.2 63.1 %all_to_all.28 = bf16[6,64,2048]{2,0,1:T(8,128)(2,1)S(1)} all-to-all(bf16[6,64,2048]{2,0,1:T(8,128)(2,1)S(1)} %copy_select_fusion), channel_id=1, replica_groups=mesh['ep'=64,'tp'=4] {'ep'}, dimensions={1} | all-to-all | bytes 3145728 | tf_op jit(solution)/shard_map/all_to_all | solution.py:115
  91.4 2.0 copy.48
  97.1 1.9 collective-permute-start
  99.1 58.8 %all-gather.3.cloned.1.call-done = bf16[24,64,2048]{2,1,0:T(8,128)(2,1)} async-done(((bf16[6,64,2048]{2,1,0:T(8,128)(2,1)}), bf16[24,64,2048]{2,1,0:T(8,128)(2,1)}) %all-gather.3.cloned.1.call-update) | async-done | bytes 6291472 | tf_op jit(solution)/shard_map/all_gather | solution.py:116
  157.9 5.1 %fusion.23 = f32[24,64,256]{2,1,0:T(8,128)S(1)} fusion(bf16[24,64,2048]{2,1,0:T(8,128)(2,1)} %all-gather.3.cloned.1.call-done, bf16[1,2048,256]{2,1,0:T(8,128)(2,1)} %param.25), kind=kOutput, calls=%fused_computation.46 | convolution fusion | flops 1610612736 | bytes 8912896 | tf_op jit(solution)/shard_map/csed,edh->cseh/dot_general | solution.py:121
  163.1 3.0 fusion.16
  166.1 3.8 %all-to-all-start.1 = ((bf16[24,64,1,256]{3,1,2,0:T(8,128)(2,1)}), bf16[24,64,1,256]{3,1,2,0:T(8,128)(2,1)S(1)}, u32[]{:S(2)}, u32[]{:S(2)}) async-start(bf16[24,64,1,256]{3,1,2,0:T(8,128)(2,1)} %fusion.16), calls=%async_computation.2 | async-start | bytes 1572864 | tf_op jit(solution)/shard_map/all_to_all | solution.py:124
  170.0 3.3 %convolution_convert_fusion = bf16[512,2048]{1,0:T(8,128)(2,1)} fusion(bf16[256,2048]{1,0:T(8,128)(2,1)S(1)} %copy-done, f32[256]{0:T(256)S(1)} %convert_element_type.223, f32[527,256]{1,0:T(8,128)S(1)} %maximum_convert_fusion, f32[512]{0:T(512)S(1)} %minimum_convert_fusion, f32[]{:T(128)S(6)} %convert_element_type.220, f32[]{:T(128)S(6)} %convert_element_type.219, ...), kind=kOutput, calls=%fused_computation.10 | convolution fusion | flops 609746944 | bytes 11668544 | tf_op jit(solution)/shard_map/dot_general | solution.py:68
  173.4 14.8 %all-to-all-done.1 = bf16[24,64,1,256]{3,1,2,0:T(8,128)(2,1)S(1)} async-done(((bf16[24,64,1,256]{3,1,2,0:T(8,128)(2,1)}), bf16[24,64,1,256]{3,1,2,0:T(8,128)(2,1)S(1)}, u32[]{:S(2)}, u32[]{:S(2)}) %all-to-all-start.1) | async-done | bytes 786464 | tf_op jit(solution)/shard_map/all_to_all | solution.py:124
  189.4 26.5 %all-gather.5.cloned.1.call-done = bf16[1,1024,2048]{2,1,0:T(8,128)(2,1)} async-done(((bf16[1,256,2048]{2,1,0:T(8,128)(2,1)}), bf16[1,1024,2048]{2,1,0:T(8,128)(2,1)}) %all-gather.5.cloned.1.call-update) | async-done | bytes 4194320 | tf_op jit(solution)/shard_map/all_gather | solution.py:119
  215.8 2.0 fusion.3
  217.8 1.8 fusion.4
  220.8 1.4 fusion.11
  222.2 2.2 copy.51
  224.4 10.9 %all-to-all-start.2 = ((bf16[6,64,2048]{2,0,1:T(8,128)(2,1)}), bf16[6,64,2048]{2,0,1:T(8,128)(2,1)}, u32[]{:S(2)}, u32[]{:S(2)}) async-start(bf16[6,64,2048]{2,0,1:T(8,128)(2,1)} %copy.51), calls=%async_computation.3 | async-start | bytes 4194304 | tf_op jit(solution)/shard_map/all_to_all | solution.py:137
  236.5 49.9 %all-to-all-done.2 = bf16[6,64,2048]{2,0,1:T(8,128)(2,1)} async-done(((bf16[6,64,2048]{2,0,1:T(8,128)(2,1)}), bf16[6,64,2048]{2,0,1:T(8,128)(2,1)}, u32[]{:S(2)}, u32[]{:S(2)}) %all-to-all-start.2) | async-done | bytes 1572896 | tf_op jit(solution)/shard_map/all_to_all | solution.py:137
  286.4 2.5 copy.52
  288.9 2.1 gather_fusion.1
  290.9 2.1 reshape.556
  293.1 3.1 %multiply_reduce_fusion.1 = bf16[96,2048]{1,0:T(8,128)(2,1)} fusion(f32[96,2,2048]{2,1,0:T(2,128)S(1)} %reshape.556, f32[96,2]{1,0:T(8,128)S(1)} %copy.53), kind=kLoop, calls=%fused_computation.31 | loop fusion | flops 589824 | bytes 1966848 | tf_op jit(solution)/shard_map/reduce_sum | solution.py:146
  (88 shorter events, 12.7 us)
Async XLA Ops:
  7.2 162.9 %copy-start = (bf16[256,2048]{1,0:T(8,128)(2,1)S(1)}, bf16[256,2048]{1,0:T(8,128)(2,1)}, u32[]{:S(2)}) copy-start(bf16[256,2048]{1,0:T(8,128)(2,1)} %param.19) | copy-start | bytes 3145732
  7.2 4.2 %copy-start.1 = (bf16[384,2048]{1,0:T(8,128)(2,1)S(1)}, bf16[384,2048]{1,0:T(8,128)(2,1)}, u32[]{:S(2)}) copy-start(bf16[384,2048]{1,0:T(8,128)(2,1)} %param.20) | copy-start | bytes 4718596
  7.2 150.7 %all-gather.3.cloned.1.call-start = ((), (), s32[]{:S(2)}) async-start(), calls=%async_computation.5 | async-start | bytes 7864320 | tf_op jit(solution)/shard_map/all_gather | solution.py:116
  13.4 10.0 %copy-start.8 = (bf16[2048]{0:T(1024)(128)(2,1)S(1)}, bf16[2048]{0:T(1024)(128)(2,1)}, u32[]{:S(2)}) copy-start(bf16[2048]{0:T(1024)(128)(2,1)} %param.21) | copy-start | bytes 12292
  93.4 0.8 copy-start.9
  93.4 1.6 copy-start.3
  93.4 122.4 %all-gather.5.cloned.1.call-start = ((), (), s32[]{:S(2)}) async-start(), calls=%async_computation.6 | async-start | bytes 5242880 | tf_op jit(solution)/shard_map/all_gather | solution.py:119
  94.2 1.4 copy-start.11
  95.6 3.5 %copy-start.14 = (bf16[256]{0:T(256)(128)(2,1)S(1)}, bf16[256]{0:T(256)(128)(2,1)}, u32[]{:S(2)}) copy-start(bf16[256]{0:T(256)(128)(2,1)} %param.18) | copy-start | bytes 1540
  96.4 0.7 copy-start.4
  97.1 72.9 %collective-permute-start = (bf16[15,256]{1,0:T(8,128)(2,1)S(1)}, bf16[15,256]{1,0:T(8,128)(2,1)S(1)}, u32[]{:S(2)}, u32[]{:S(2)}) collective-permute-start(bf16[15,256]{1,0:T(8,128)(2,1)S(1)} %slice.135), channel_id=1, source_target_pairs={{0,4},{4,8},{8,12},{12,16},{16,20},{20,24},{24,28},{28,32},{32,36}... | collective-permute-start | bytes 23048 | tf_op jit(solution)/shard_map/ppermute | solution.py:13
  157.9 5.1 %copy-start.10 = (bf16[24,64,2048]{2,1,0:T(8,128)(2,1)S(1)}, bf16[24,64,2048]{2,1,0:T(8,128)(2,1)}, u32[]{:S(2)}) copy-start(bf16[24,64,2048]{2,1,0:T(8,128)(2,1)} %all-gather.3.cloned.1.call-done) | copy-start | bytes 18874372
  157.9 5.1 %copy-start.12 = (bf16[1,2048,256]{2,1,0:T(8,128)(2,1)S(1)}, bf16[1,2048,256]{2,1,0:T(8,128)(2,1)}, u32[]{:S(2)}) copy-start(bf16[1,2048,256]{2,1,0:T(8,128)(2,1)} %param.26) | copy-start | bytes 3145732
  163.1 6.9 %copy-start.5 = (bf16[512,256]{1,0:T(8,128)(2,1)S(1)}, bf16[512,256]{1,0:T(8,128)(2,1)}, u32[]{:S(2)}) copy-start(bf16[512,256]{1,0:T(8,128)(2,1)} %copy-done.4) | copy-start | bytes 786436
  166.1 4.0 %copy-start.13 = (bf16[1,256,256]{2,1,0:T(8,128)(2,1)S(1)}, bf16[1,256,256]{2,1,0:T(8,128)(2,1)}, u32[]{:S(2)}) copy-start(bf16[1,256,256]{2,1,0:T(8,128)(2,1)} %param.17) | copy-start | bytes 393220
  166.1 22.1 %all-to-all-start.1 = ((bf16[24,64,1,256]{3,1,2,0:T(8,128)(2,1)}), bf16[24,64,1,256]{3,1,2,0:T(8,128)(2,1)S(1)}, u32[]{:S(2)}, u32[]{:S(2)}) async-start(bf16[24,64,1,256]{3,1,2,0:T(8,128)(2,1)} %fusion.16), calls=%async_computation.2 | async-start | bytes 1572864 | tf_op jit(solution)/shard_map/all_to_all | solution.py:124
  169.9 126.4 %reduce-scatter.2.cloned.1.call-start = ((), (), s32[]{:S(2)}) async-start(), calls=%async_computation.4 | async-start | bytes 2621440 | tf_op jit(solution)/shard_map/reduce_scatter | solution.py:67
  215.8 3.8 %copy-start.2 = (bf16[1,1024,2048]{2,1,0:T(8,128)(2,1)S(1)}, bf16[1,1024,2048]{2,1,0:T(8,128)(2,1)}, u32[]{:S(2)}) copy-start(bf16[1,1024,2048]{2,1,0:T(8,128)(2,1)} %all-gather.5.cloned.1.call-done) | copy-start | bytes 12582916
  224.4 10.9 %copy-start.7 = (bf16[2048,4]{0,1:T(4,128)(2,1)S(1)}, bf16[2048,4]{0,1:T(4,128)(2,1)}, u32[]{:S(2)}) copy-start(bf16[2048,4]{0,1:T(4,128)(2,1)} %param.22) | copy-start | bytes 49156
  224.4 11.2 %copy-start.6 = (bf16[2048,64]{0,1:T(8,128)(2,1)S(1)}, bf16[2048,64]{0,1:T(8,128)(2,1)}, u32[]{:S(2)}) copy-start(bf16[2048,64]{0,1:T(8,128)(2,1)} %param.23) | copy-start | bytes 786436
  224.4 62.0 %all-to-all-start.2 = ((bf16[6,64,2048]{2,0,1:T(8,128)(2,1)}), bf16[6,64,2048]{2,0,1:T(8,128)(2,1)}, u32[]{:S(2)}, u32[]{:S(2)}) async-start(bf16[6,64,2048]{2,0,1:T(8,128)(2,1)} %copy.51), calls=%async_computation.3 | async-start | bytes 4194304 | tf_op jit(solution)/shard_map/all_to_all | solution.py:137
Sparse Core Ops, SparseCore 0:
  93.5 64.3 all-gather.2
  159.7 56.0 all-gather.4
  219.0 31.9 reduce-scatter.1
where the time goes:
time: 303 us
  waiting for transfers between devices  151 us (50%)
  blocking collectives  63.1 us (21%)
  local copies, waits for them, and re-layouts  27.7 us (9%)
  matrix products  18 us (6%)
  starting transfers between devices  16.7 us (6%)
  between operations  14.2 us (5%)
  other arithmetic  12.1 us (4%)
    all_to_all x1, blocking collectives, expert_half(): lax.all_to_all(sending, 'ep', split_axis=1, concat_axis=1, tiled=True)  63.1 us
    all_gather x1, waiting for transfers between devices, expert_half(): received = lax.all_gather(arrived, 'tp', axis=0, tiled=True)  58.8 us
    all_to_all x1, waiting for transfers between devices, expert_half(): lax.all_to_all(summed, 'ep', split_axis=1, concat_axis=1, tiled=True)  49.9 us
    all_gather x1, waiting for transfers between devices, expert_half(): down_whole = lax.all_gather(down_weight, 'tp', axis=1, tiled=True)  26.5 us
    all_to_all x1, waiting for transfers between devices, expert_half(): lax.all_to_all(hidden, 'tp', split_axis=0, concat_axis=3, tiled=True)  14.8 us
    all_to_all x1, starting transfers between devices, expert_half(): lax.all_to_all(summed, 'ep', split_axis=1, concat_axis=1, tiled=True)  10.9 us
    scatter x1, local copies, waits for them, and re-layouts, dispatch_rows(): table.at[slot_index.reshape(-1), flat.reshape(-1)]  9.28 us
  transfers between devices with their start and end apart: 6, of which 4 were waited for; matrix products, arithmetic and copies ran while one was open for 11% of the time, Pallas kernels for 0%

commit v1 on v0

--- a/solution.py
+++ b/solution.py
@@ -116,7 +116,9 @@
     received = lax.all_gather(arrived, "tp", axis=0, tiled=True)
     held = gate_weight.shape[0]
     model = received.shape[2]
-    down_whole = lax.all_gather(down_weight, "tp", axis=1, tiled=True)
+    down_whole = jnp.concatenate(
+        lax.all_to_all(jnp.stack([down_weight] * lax.axis_size("tp")), "tp", 0, 0), axis=1
+    )
     all_slots = received.reshape(received.shape[0], -1, held, model)
     gate = jnp.einsum("csed,edh->cseh", all_slots, gate_weight, preferred_element_type=jnp.float32)
     upward = jnp.einsum("csed,edh->cseh", all_slots, up_weight, preferred_element_type=jnp.float32)

time: 303 us -> 343 us (1.13)
  waiting for transfers between devices: 151 us -> 168 us
  blocking collectives: 63.1 us -> 78.8 us
    all_to_all x1, waiting for transfers between devices: 14.8 us -> 50.6 us  [expert_half(): lax.all_to_all(jnp.stack([down_weight] * lax.axis_size('tp')), 'tp', 0, 0)]
    all_gather x1 -> x0, waiting for transfers between devices: 26.5 us -> none  [expert_half(): down_whole = lax.all_gather(down_weight, 'tp', axis=1, tiled=True)]
    all_to_all x0 -> x1, blocking collectives: none -> 15.7 us  [expert_half(): lax.all_to_all(hidden, 'tp', split_axis=0, concat_axis=3, tiled=True)]
    all_gather x1, waiting for transfers between devices: 58.8 us -> 64.5 us  [expert_half(): received = lax.all_gather(arrived, 'tp', axis=0, tiled=True)]
  transfers between devices with their start and end apart: 6 -> 5, of which waited for: 4 -> 4; matrix products, arithmetic and copies ran while one was open for 11% -> 9% of each run, Pallas kernels for 0% -> 0%
where the time goes in v1:
time: 343 us; the launch traced here: 342 us
  waiting for transfers between devices  168 us (49%)
  blocking collectives  78.8 us (23%)
  local copies, waits for them, and re-layouts  28.5 us (8%)
  matrix products  20.3 us (6%)
  starting transfers between devices  18 us (5%)
  between operations  14.5 us (4%)
  other arithmetic  13.8 us (4%)
    all_gather x1, waiting for transfers between devices, expert_half(): received = lax.all_gather(arrived, 'tp', axis=0, tiled=True)  64.5 us
    all_to_all x1, blocking collectives, expert_half(): lax.all_to_all(sending, 'ep', split_axis=1, concat_axis=1, tiled=True)  63.1 us
    all_to_all x1, waiting for transfers between devices, expert_half(): lax.all_to_all(jnp.stack([down_weight] * lax.axis_size('tp')), 'tp', 0, 0)  50.6 us
    all_to_all x1, waiting for transfers between devices, expert_half(): lax.all_to_all(summed, 'ep', split_axis=1, concat_axis=1, tiled=True)  49.9 us
    all_to_all x1, blocking collectives, expert_half(): lax.all_to_all(hidden, 'tp', split_axis=0, concat_axis=3, tiled=True)  15.7 us
    all_to_all x1, starting transfers between devices, expert_half(): lax.all_to_all(summed, 'ep', split_axis=1, concat_axis=1, tiled=True)  10.9 us
    scatter x1, local copies, waits for them, and re-layouts, dispatch_rows(): table.at[slot_index.reshape(-1), flat.reshape(-1)]  9.28 us
    dot_general x4, matrix products, expert_half(): jnp.einsum('cseh,ehd->csed', swapped[:, :, :, part * hid_part:(part + 1)...  7.2 us
  transfers between devices with their start and end apart: 5, of which 4 were waited for; matrix products, arithmetic and copies ran while one was open for 9% of the time, Pallas kernels for 0%

profile of v1, /device:TPU:8, one launch (start us, length us, event | category | flops | bytes accessed | tf_op | source)
XLA Modules:
  0.0 342.1 jit_solution(14248207960212915643)
XLA Ops:
  11.3 2.0 convert_element_type.227
  13.9 9.3 %scatter_fusion = s32[6,64]{1,0:T(8,128)S(1)} fusion(s32[6,64]{1,0:T(8,128)S(1)} %broadcast_in_dim.11, s32[192]{0:T(256)S(1)} %bitcast.131, s32[192]{0:T(256)S(1)} %and_select_fusion.1), kind=kCustom, calls=%fused_computation.2 | custom fusion | bytes 3840 | tf_op jit(solution)/shard_map/scatter | solution.py:91
  24.8 2.5 gather_fusion
  28.2 63.1 %all_to_all.33 = bf16[6,64,2048]{2,0,1:T(8,128)(2,1)S(1)} all-to-all(bf16[6,64,2048]{2,0,1:T(8,128)(2,1)S(1)} %copy_select_fusion), channel_id=1, replica_groups=mesh['ep'=64,'tp'=4] {'ep'}, dimensions={1} | all-to-all | bytes 3145728 | tf_op jit(solution)/shard_map/all_to_all | solution.py:115
  91.4 2.0 copy.48
  93.4 64.5 %all-gather.2.cloned.1.call-done = bf16[24,64,2048]{2,1,0:T(8,128)(2,1)} async-done(((bf16[6,64,2048]{2,1,0:T(8,128)(2,1)}), bf16[24,64,2048]{2,1,0:T(8,128)(2,1)}) %all-gather.2.cloned.1.call-update) | async-done | bytes 6291472 | tf_op jit(solution)/shard_map/all_gather | solution.py:116
  157.9 4.8 %fusion.23 = f32[24,64,256]{2,1,0:T(8,128)S(1)} fusion(bf16[24,64,2048]{2,1,0:T(8,128)(2,1)} %all-gather.2.cloned.1.call-done, bf16[1,2048,256]{2,1,0:T(8,128)(2,1)S(1)} %copy-done.9), kind=kOutput, calls=%fused_computation.46 | convolution fusion | flops 1610612736 | bytes 8912896 | tf_op jit(solution)/shard_map/csed,edh->cseh/dot_general | solution.py:123
  162.8 2.1 fusion.16
  164.9 15.7 %all_to_all.34 = bf16[24,64,1,256]{3,1,2,0:T(8,128)(2,1)S(1)} all-to-all(bf16[24,64,1,256]{3,1,2,0:T(8,128)(2,1)S(1)} %fusion.16), channel_id=1, replica_groups=mesh['ep'=64,'tp'=4] {'tp'}, dimensions={0} | all-to-all | bytes 1572864 | tf_op jit(solution)/shard_map/all_to_all | solution.py:126
  180.6 2.5 stack.2
  183.1 5.0 %all-to-all-start.2 = ((bf16[4,1,256,2048]{3,2,1,0:T(8,128)(2,1)}), bf16[4,1,256,2048]{3,2,1,0:T(8,128)(2,1)}, u32[]{:S(2)}, u32[]{:S(2)}) async-start(bf16[4,1,256,2048]{3,2,1,0:T(8,128)(2,1)} %stack.2), calls=%async_computation.3 | async-start | bytes 8388608 | tf_op jit(solution)/shard_map/all_to_all | solution.py:120
  188.3 2.2 fusion
  190.6 2.0 fusion.17
  192.7 1.9 collective-permute-start
  194.7 2.9 collective-permute-done
  197.7 3.2 convolution_convert_fusion
  202.2 50.6 %all-to-all-done.2 = bf16[4,1,256,2048]{3,2,1,0:T(8,128)(2,1)} async-done(((bf16[4,1,256,2048]{3,2,1,0:T(8,128)(2,1)}), bf16[4,1,256,2048]{3,2,1,0:T(8,128)(2,1)}, u32[]{:S(2)}, u32[]{:S(2)}) %all-to-all-start.2) | async-done | bytes 4194336 | tf_op jit(solution)/shard_map/all_to_all | solution.py:120
  261.4 2.2 copy.51
  263.6 10.9 %all-to-all-start.3 = ((bf16[6,64,2048]{2,0,1:T(8,128)(2,1)}), bf16[6,64,2048]{2,0,1:T(8,128)(2,1)}, u32[]{:S(2)}, u32[]{:S(2)}) async-start(bf16[6,64,2048]{2,0,1:T(8,128)(2,1)} %copy.51), calls=%async_computation.4 | async-start | bytes 4194304 | tf_op jit(solution)/shard_map/all_to_all | solution.py:139
  275.6 49.9 %all-to-all-done.3 = bf16[6,64,2048]{2,0,1:T(8,128)(2,1)} async-done(((bf16[6,64,2048]{2,0,1:T(8,128)(2,1)}), bf16[6,64,2048]{2,0,1:T(8,128)(2,1)}, u32[]{:S(2)}, u32[]{:S(2)}) %all-to-all-start.3) | async-done | bytes 1572896 | tf_op jit(solution)/shard_map/all_to_all | solution.py:139
  325.6 2.5 copy.52
  328.0 2.0 gather_fusion.1
  330.1 2.1 reshape.563
  332.2 3.1 multiply_reduce_fusion.1
  (83 shorter events, 18.4 us)
Async XLA Ops:
  7.2 190.5 %copy-start = (bf16[256,2048]{1,0:T(8,128)(2,1)S(1)}, bf16[256,2048]{1,0:T(8,128)(2,1)}, u32[]{:S(2)}) copy-start(bf16[256,2048]{1,0:T(8,128)(2,1)} %param.19) | copy-start | bytes 3145732
  7.2 4.2 %copy-start.1 = (bf16[384,2048]{1,0:T(8,128)(2,1)S(1)}, bf16[384,2048]{1,0:T(8,128)(2,1)}, u32[]{:S(2)}) copy-start(bf16[384,2048]{1,0:T(8,128)(2,1)} %param.20) | copy-start | bytes 4718596
  7.2 150.7 %all-gather.2.cloned.1.call-start = ((), (), s32[]{:S(2)}) async-start(), calls=%async_computation.6 | async-start | bytes 7864320 | tf_op jit(solution)/shard_map/all_gather | solution.py:116
  13.4 10.0 %copy-start.6 = (bf16[2048]{0:T(1024)(128)(2,1)S(1)}, bf16[2048]{0:T(1024)(128)(2,1)}, u32[]{:S(2)}) copy-start(bf16[2048]{0:T(1024)(128)(2,1)} %param.21) | copy-start | bytes 12292
  91.4 66.6 %copy-start.9 = (bf16[1,2048,256]{2,1,0:T(8,128)(2,1)S(1)}, bf16[1,2048,256]{2,1,0:T(8,128)(2,1)}, u32[]{:S(2)}) copy-start(bf16[1,2048,256]{2,1,0:T(8,128)(2,1)} %param.25) | copy-start | bytes 3145732
  157.9 4.8 %copy-start.8 = (bf16[24,64,2048]{2,1,0:T(8,128)(2,1)S(1)}, bf16[24,64,2048]{2,1,0:T(8,128)(2,1)}, u32[]{:S(2)}) copy-start(bf16[24,64,2048]{2,1,0:T(8,128)(2,1)} %all-gather.2.cloned.1.call-done) | copy-start | bytes 18874372
  157.9 4.9 %copy-start.10 = (bf16[1,2048,256]{2,1,0:T(8,128)(2,1)S(1)}, bf16[1,2048,256]{2,1,0:T(8,128)(2,1)}, u32[]{:S(2)}) copy-start(bf16[1,2048,256]{2,1,0:T(8,128)(2,1)} %param.26) | copy-start | bytes 3145732
  164.9 15.7 %copy-start.3 = (bf16[1,256,2048]{2,1,0:T(8,128)(2,1)S(1)}, bf16[1,256,2048]{2,1,0:T(8,128)(2,1)}, u32[]{:S(2)}) copy-start(bf16[1,256,2048]{2,1,0:T(8,128)(2,1)} %param.27) | copy-start | bytes 3145732
  183.1 5.2 %copy-start.7 = (bf16[2048]{0:T(1024)(128)(2,1)S(1)}, bf16[2048]{0:T(1024)(128)(2,1)}, u32[]{:S(2)}) copy-start(bf16[2048]{0:T(1024)(128)(2,1)} %param.15) | copy-start | bytes 12292
  183.1 69.7 %all-to-all-start.2 = ((bf16[4,1,256,2048]{3,2,1,0:T(8,128)(2,1)}), bf16[4,1,256,2048]{3,2,1,0:T(8,128)(2,1)}, u32[]{:S(2)}, u32[]{:S(2)}) async-start(bf16[4,1,256,2048]{3,2,1,0:T(8,128)(2,1)} %stack.2), calls=%async_computation.3 | async-start | bytes 8388608 | tf_op jit(solution)/shard_map/all_to_all | solution.py:120
  188.1 147.2 %reduce-scatter.2.cloned.1.call-start = ((), (), s32[]{:S(2)}) async-start(), calls=%async_computation.5 | async-start | bytes 2621440 | tf_op jit(solution)/shard_map/reduce_scatter | solution.py:67
  188.3 2.3 copy-start.2
  190.6 4.1 %copy-start.12 = (bf16[256]{0:T(256)(128)(2,1)S(1)}, bf16[256]{0:T(256)(128)(2,1)}, u32[]{:S(2)}) copy-start(bf16[256]{0:T(256)(128)(2,1)} %param.18) | copy-start | bytes 1540
  190.6 7.1 %copy-start.11 = (bf16[1,256,256]{2,1,0:T(8,128)(2,1)S(1)}, bf16[1,256,256]{2,1,0:T(8,128)(2,1)}, u32[]{:S(2)}) copy-start(bf16[1,256,256]{2,1,0:T(8,128)(2,1)} %param.17) | copy-start | bytes 393220
  192.7 5.0 %collective-permute-start = (bf16[15,256]{1,0:T(8,128)(2,1)S(1)}, bf16[15,256]{1,0:T(8,128)(2,1)S(1)}, u32[]{:S(2)}, u32[]{:S(2)}) collective-permute-start(bf16[15,256]{1,0:T(8,128)(2,1)S(1)} %slice.135), channel_id=1, source_target_pairs={{0,4},{4,8},{8,12},{12,16},{16,20},{20,24},{24,28},{28,32},{32,36}... | collective-permute-start | bytes 23048 | tf_op jit(solution)/shard_map/ppermute | solution.py:13
  263.6 10.9 %copy-start.5 = (bf16[2048,4]{0,1:T(4,128)(2,1)S(1)}, bf16[2048,4]{0,1:T(4,128)(2,1)}, u32[]{:S(2)}) copy-start(bf16[2048,4]{0,1:T(4,128)(2,1)} %param.22) | copy-start | bytes 49156
  263.6 11.1 %copy-start.4 = (bf16[2048,64]{0,1:T(8,128)(2,1)S(1)}, bf16[2048,64]{0,1:T(8,128)(2,1)}, u32[]{:S(2)}) copy-start(bf16[2048,64]{0,1:T(8,128)(2,1)} %param.23) | copy-start | bytes 786436
  263.6 62.0 %all-to-all-start.3 = ((bf16[6,64,2048]{2,0,1:T(8,128)(2,1)}), bf16[6,64,2048]{2,0,1:T(8,128)(2,1)}, u32[]{:S(2)}, u32[]{:S(2)}) async-start(bf16[6,64,2048]{2,0,1:T(8,128)(2,1)} %copy.51), calls=%async_computation.4 | async-start | bytes 4194304 | tf_op jit(solution)/shard_map/all_to_all | solution.py:139
Sparse Core Ops, SparseCore 0:
  93.5 64.3 all-gather.1
  201.1 51.0 reduce-scatter.1
